TPU v7x, 32 devices: a whole 2x2x4 slice. The times are simulated.
32 devices in a mesh: rep: 2 (over x), fs: 8 (over z, y), tp: 2 (over core).
Axes of the slice: x: 2, y: 2, z: 4, core: 2. Of those that a mesh axis runs over, the one named last changes fastest.
Arguments:
- activations: bfloat16 [16384, 1024], P(('rep', 'fs', 'tp')), may hold values from -8 to 8
- mixer_gain: float32 [1024], replicated, may hold values from 0.1 to 1.9
- query_weight: bfloat16 [1024, 256], P('fs', 'tp'), may hold values from -0.1875 to 0.1875
- key_weight: bfloat16 [1024, 256], P('fs', 'tp'), may hold values from -0.1875 to 0.1875
- value_weight: bfloat16 [1024, 512], P('fs', 'tp'), may hold values from -0.1875 to 0.1875
- rank_weight: bfloat16 [1024, 16], replicated, may hold values from -0.1875 to 0.1875
- decay_gate_weight: bfloat16 [16, 256], P(None, 'tp'), may hold values from -1.5 to 1.5
- decay_gate_bias: float32 [256], P('tp'), may hold values from -1.5 to 8
- head_gain: float32 [256], replicated, may hold values from 0.1 to 1.9
- output_weight: bfloat16 [512, 1024], P('tp', 'fs'), may hold values from -0.25 to 0.25
- ffn_gain: float32 [1024], replicated, may hold values from 0.1 to 1.9
- gate_weight: bfloat16 [1024, 2816], P('fs', 'tp'), may hold values from -0.1875 to 0.1875
- up_weight: bfloat16 [1024, 2816], P('fs', 'tp'), may hold values from -0.1875 to 0.1875
- down_weight: bfloat16 [2816, 1024], P('tp', 'fs'), may hold values from -0.109375 to 0.109375
Outputs:
- result: bfloat16 [16384, 1024], P(('rep', 'fs', 'tp'))
All inputs are finite; a program needn't handle non-finite values.
Results may differ from a plain program's by a relative error of at most 0.0056.
Values may be sent and summed in bfloat16 or wider, within the bound.
No kernel may reach another device: no remote copies, remote signals or barrier semaphores. Data moves between devices by JAX's collectives and lax.ppermute only.
A program may use at most 64 MiB of HBM per device.

v0:
```python
import jax
import jax.numpy as jnp
from jax import lax
from jax.sharding import PartitionSpec as P

DK = 128
DV = 256
BLOCK = 64
epsilon = 1e-06
decay_softness = 16.0
highest = lax.Precision.HIGHEST


def rms_scale(values, gains):
    return values * lax.rsqrt(jnp.mean(values * values, axis=-1, keepdims=True) + epsilon) * gains


def linear_attention(queries, keys_all, values_all, decay_logarithm, head_count):
    length = queries.shape[0]
    number = length // BLOCK
    halfway = BLOCK // 2
    causal = jnp.tril(jnp.ones((BLOCK, BLOCK), bool))

    def to_blocks(matrix):
        return matrix.astype(jnp.float32).reshape(
            number, BLOCK, head_count, matrix.shape[1] // head_count
        )

    block_query = to_blocks(queries)
    block_key = to_blocks(keys_all)
    block_value = to_blocks(values_all)
    cumulative = jnp.cumsum(to_blocks(decay_logarithm), axis=1)
    middle = cumulative[:, halfway - 1 : halfway]
    query_local = block_query * jnp.exp(cumulative - middle)
    key_local = block_key * jnp.exp(middle - cumulative)
    scores = jnp.einsum("nthd,nshd->nhts", query_local, key_local, precision=highest)
    scores = jnp.where(causal[None, None], scores, 0.0)
    within = jnp.einsum("nhts,nshv->nthv", scores, block_value, precision=highest)
    lasting = cumulative[:, -1]
    update = jnp.einsum(
        "nshd,nshv->nhdv",
        block_key * jnp.exp(lasting[:, None] - cumulative),
        block_value,
        precision=highest,
    )

    def advance(memory, inputs):
        fade, addition = inputs
        return (jnp.exp(fade)[:, :, None] * memory + addition, memory)

    key_width = queries.shape[1] // head_count
    value_width = values_all.shape[1] // head_count
    initial = jnp.zeros((head_count, key_width, value_width), jnp.float32)
    earlier = lax.scan(advance, initial, (lasting, update))[1]
    carried = jnp.einsum(
        "nthd,nhdv->nthv", block_query * jnp.exp(cumulative), earlier, precision=highest
    )
    return (within + carried).reshape(length, head_count, value_width)


def project_inputs(source, weight):
    return jnp.dot(source, weight, preferred_element_type=jnp.float32)


def local(
    activations,
    mixer_gain,
    query_weight,
    key_weight,
    value_weight,
    rank_weight,
    decay_gate_weight,
    decay_gate_bias,
    head_gain,
    output_weight,
    ffn_gain,
    gate_weight,
    up_weight,
    down_weight,
):
    residual = activations.astype(jnp.float32)
    normed = rms_scale(residual, mixer_gain).astype(jnp.bfloat16)
    rank_slice = project_inputs(normed, rank_weight).astype(jnp.bfloat16)
    sequence, rank_slices_gathered = (
        lax.all_gather(normed, "tp", axis=0, tiled=True),
        lax.all_gather(rank_slice, "tp", axis=0, tiled=True),
    )
    length = sequence.shape[0]
    query_full, key_full, value_full = (
        lax.all_gather(query_weight, "fs", axis=0, tiled=True),
        lax.all_gather(key_weight, "fs", axis=0, tiled=True),
        lax.all_gather(value_weight, "fs", axis=0, tiled=True),
    )
    queries = project_inputs(sequence, query_full).astype(jnp.bfloat16)
    keys_all = project_inputs(sequence, key_full).astype(jnp.bfloat16)
    values_all = project_inputs(sequence, value_full).astype(jnp.bfloat16)
    decay_logarithm = (
        jax.nn.log_sigmoid(
            project_inputs(rank_slices_gathered, decay_gate_weight) + decay_gate_bias
        )
        / decay_softness
    )
    head_count = query_weight.shape[1] // DK
    attended = linear_attention(queries, keys_all, values_all, decay_logarithm, head_count)
    head_rows = rms_scale(attended, head_gain).astype(jnp.bfloat16).reshape(length, head_count * DV)
    own_rows = lax.all_to_all(head_rows, "tp", split_axis=0, concat_axis=1, tiled=True)
    tall_out = lax.all_gather(output_weight, "tp", axis=0, tiled=True)
    whole_out = lax.all_gather(tall_out, "fs", axis=1, tiled=True)
    mixed = residual + project_inputs(own_rows, whole_out)
    ffn_normed = rms_scale(mixed, ffn_gain).astype(jnp.bfloat16)
    ffn_sequence = lax.all_gather(ffn_normed, "tp", axis=0, tiled=True)
    gate_full, up_full = (
        lax.all_gather(gate_weight, "fs", axis=0, tiled=True),
        lax.all_gather(up_weight, "fs", axis=0, tiled=True),
    )
    down_full = lax.all_gather(down_weight, "fs", axis=1, tiled=True)
    hidden = (
        jax.nn.silu(project_inputs(ffn_sequence, gate_full)) * project_inputs(ffn_sequence, up_full)
    ).astype(jnp.bfloat16)
    result = mixed + lax.psum_scatter(
        project_inputs(hidden, down_full).astype(jnp.bfloat16),
        "tp",
        scatter_dimension=0,
        tiled=True,
    ).astype(jnp.float32)
    return result.astype(jnp.bfloat16)


def solution(mesh):
    in_specs = (
        P(("rep", "fs", "tp"), None),
        P(),
        P("fs", "tp"),
        P("fs", "tp"),
        P("fs", "tp"),
        P(),
        P(None, "tp"),
        P("tp"),
        P(),
        P("tp", "fs"),
        P(),
        P("fs", "tp"),
        P("fs", "tp"),
        P("tp", "fs"),
    )
    out_specs = P(("rep", "fs", "tp"), None)
    return jax.shard_map(local, mesh=mesh, in_specs=in_specs, out_specs=out_specs, check_vma=False)
```

profile of v0, /device:TPU:0, one launch (start us, length us, event | category | flops | bytes accessed | tf_op | source)
XLA Modules:
  0.0 369.9 jit_solution(17549334003282702146)
XLA Ops:
  6.5 1.5 fusion.2
  8.1 2.5 fusion.4
  10.7 2.2 all_gather.38
  13.0 1.6 convolution_convert_fusion.3
  14.6 2.1 all_gather.36
  16.8 0.5 fusion.12
  17.2 0.3 fusion.24
  17.6 32.6 %all_gather.37 = bf16[1024,128]{1,0:T(8,128)(2,1)S(1)} all-gather(bf16[128,128]{1,0:T(8,128)(2,1)S(1)} %copy-done.8), channel_id=1, replica_groups=mesh['rep'=2,'fs'=8,'tp'=2] {'fs'}, dimensions={0}, use_global_device_ids=true | all-gather | bytes 294912 | tf_op jit(solution)/shard_map/all_gather | solution.py:91
  50.2 31.1 %all_gather.35 = bf16[1024,128]{1,0:T(8,128)(2,1)S(1)} all-gather(bf16[128,128]{1,0:T(8,128)(2,1)S(1)} %copy-done.9), channel_id=1, replica_groups=mesh['rep'=2,'fs'=8,'tp'=2] {'fs'}, dimensions={0}, use_global_device_ids=true | all-gather | bytes 294912 | tf_op jit(solution)/shard_map/all_gather | solution.py:90
  81.3 31.3 %all_gather.34 = bf16[1024,256]{1,0:T(8,128)(2,1)S(1)} all-gather(bf16[128,256]{1,0:T(8,128)(2,1)S(1)} %copy-done.7), channel_id=1, replica_groups=mesh['rep'=2,'fs'=8,'tp'=2] {'fs'}, dimensions={0}, use_global_device_ids=true | all-gather | bytes 589824 | tf_op jit(solution)/shard_map/all_gather | solution.py:92
  112.6 2.4 convolution_convert_fusion.1
  115.1 0.7 convolution_convert_fusion.2
  115.8 1.6 fusion.14
  117.4 0.7 convolution_convert_fusion
  118.1 1.1 convolution_bitcast_fusion
  119.2 12.6 %while.13 = (s32[]{:T(128)}, f32[1,128,256]{2,1,0:T(8,128)S(1)}, f32[16,1,128,256]{3,2,1,0:T(8,128)}, f32[16,1,128]{2,1,0:T(1,128)S(1)}, f32[16,1,128,256]{3,2,1,0:T(8,128)S(1)}, /*index=5*/s32[]{:T(128)}, s32[]{:T(128)}) while((s32[]{:T(128)}, f32[1,128,256]{2,1,0:T(8,128)S(1)}, f32[16,1,128,256]{3,2,1,0:T(8,128)}, ...), condition=%wide.region_3.4_spmd.clone, body=%wide.region_2.3_spmd.clone.sunk | while | flops 131075 | bytes 657504 | solution.py:54
  119.2 0.7 bitcast_dynamic-update-slice_fusion.2
  119.9 0.1 bitcast_add_fusion.2
  120.0 0.7 bitcast_dynamic-update-slice_fusion.2
  120.7 0.1 bitcast_add_fusion.2
  120.8 0.7 bitcast_dynamic-update-slice_fusion.2
  121.4 0.1 bitcast_add_fusion.2
  121.6 0.7 bitcast_dynamic-update-slice_fusion.2
  122.2 0.1 bitcast_add_fusion.2
  122.3 0.7 bitcast_dynamic-update-slice_fusion.2
  123.0 0.1 bitcast_add_fusion.2
  123.1 0.7 bitcast_dynamic-update-slice_fusion.2
  123.8 0.1 bitcast_add_fusion.2
  123.9 0.6 bitcast_dynamic-update-slice_fusion.2
  124.6 0.1 bitcast_add_fusion.2
  124.7 0.7 bitcast_dynamic-update-slice_fusion.2
  125.4 0.1 bitcast_add_fusion.2
  125.5 0.7 bitcast_dynamic-update-slice_fusion.2
  126.2 0.1 bitcast_add_fusion.2
  126.3 0.7 bitcast_dynamic-update-slice_fusion.2
  127.1 0.7 bitcast_dynamic-update-slice_fusion.2
  127.7 0.1 bitcast_add_fusion.2
  127.9 0.7 bitcast_dynamic-update-slice_fusion.2
  128.7 0.7 bitcast_dynamic-update-slice_fusion.2
  129.4 0.7 bitcast_dynamic-update-slice_fusion.2
  130.2 0.7 bitcast_dynamic-update-slice_fusion.2
  131.0 0.7 bitcast_dynamic-update-slice_fusion.2
  131.8 2.2 convolution_select_fusion
  134.1 3.0 fusion.5
  137.1 0.7 fusion.10
  137.8 0.3 copy.33
  138.3 0.9 multiply_convert_fusion.2
  139.2 3.5 all-to-all-start
  142.8 1.7 all-to-all-done
  144.4 0.8 copy-done.3
  145.2 2.2 multiply_reduce_fusion
  147.5 1.2 multiply_convert_fusion.1
  148.7 0.5 all-gather.13.cloned.1.call-update
  149.3 0.5 all-gather.15.cloned.1.call-update
  149.9 0.5 all-gather.17.cloned.1.call-update
  150.4 0.2 reduce-scatter.2.cloned.1.call-start
  150.7 10.0 %all-gather.11.cloned.1.call-done = bf16[1024,1024]{1,0:T(8,128)(2,1)} async-done(((bf16[512,1024]{1,0:T(8,128)(2,1)}), bf16[1024,1024]{1,0:T(8,128)(2,1)}) %all-gather.11.cloned.1.call-update) | async-done | bytes 2097168 | tf_op jit(solution)/shard_map/all_gather | solution.py:111
  160.7 60.5 %all-gather.13.cloned.1.call-done = bf16[1024,1408]{1,0:T(8,128)(2,1)} async-done(((bf16[128,1408]{1,0:T(8,128)(2,1)}), bf16[1024,1408]{1,0:T(8,128)(2,1)}) %all-gather.13.cloned.1.call-update) | async-done | bytes 2883600 | tf_op jit(solution)/shard_map/all_gather | solution.py:113
  221.2 8.3 %fusion.27 = f32[1024,1408]{1,0:T(8,128)} fusion(bf16[1024,1024]{1,0:T(8,128)(2,1)} %all-gather.11.cloned.1.call-done, bf16[1024,1408]{1,0:T(8,128)(2,1)} %all-gather.13.cloned.1.call-done), kind=kOutput, calls=%fused_computation.58 | convolution fusion | flops 2952790016 | bytes 10747904 | tf_op jit(solution)/shard_map/dot_general | solution.py:62
  229.6 49.6 %all-gather.15.cloned.1.call-done = bf16[1024,1408]{1,0:T(8,128)(2,1)} async-done(((bf16[128,1408]{1,0:T(8,128)(2,1)}), bf16[1024,1408]{1,0:T(8,128)(2,1)}) %all-gather.15.cloned.1.call-update) | async-done | bytes 2883600 | tf_op jit(solution)/shard_map/all_gather | solution.py:114
  279.2 60.1 %all-gather.17.cloned.1.call-done = bf16[1408,1024]{1,0:T(8,128)(2,1)} async-done(((bf16[1408,128]{1,0:T(8,128)(2,1)}), bf16[1408,1024]{1,0:T(8,128)(2,1)}) %all-gather.17.cloned.1.call-update) | async-done | bytes 2883600 | tf_op jit(solution)/shard_map/all_gather | solution.py:116
  339.3 13.1 %fusion.8 = bf16[1024,1024]{1,0:T(8,128)(2,1)} fusion(bf16[1408,1024]{1,0:T(8,128)(2,1)} %all-gather.17.cloned.1.call-done, f32[1024,1408]{1,0:T(8,128)} %fusion.27, bf16[1024,1024]{1,0:T(8,128)(2,1)} %all-gather.11.cloned.1.call-done, bf16[1024,1408]{1,0:T(8,128)(2,1)} %all-gather.15.cloned.1.call-done), kind=kOutput, calls=%fused_computation.18 | convolution fusion | flops 5915279360 | bytes 15728640 | tf_op jit(solution)/shard_map/dot_general | solution.py:62
  352.4 8.1 %reduce-scatter.2.cloned.1.call-done = bf16[512,1024]{1,0:T(8,128)(2,1)} async-done(((bf16[1024,1024]{1,0:T(8,128)(2,1)}), bf16[512,1024]{1,0:T(8,128)(2,1)}) %reduce-scatter.2.cloned.1.call-update) | async-done | bytes 1048592 | tf_op jit(solution)/shard_map/reduce_scatter | solution.py:120
  360.5 2.5 add_convert_fusion
  (71 shorter events, 1.2 us)
Async XLA Ops:
  6.5 6.4 %copy-start = (bf16[1024,16]{0,1:T(8,128)(2,1)S(1)}, bf16[1024,16]{0,1:T(8,128)(2,1)}, u32[]{:S(2)}) copy-start(bf16[1024,16]{0,1:T(8,128)(2,1)} %param.21) | copy-start | bytes 98308
  6.5 106.0 %all-gather.7.cloned.1.call-start = ((), (), s32[]{:S(2)}) async-start(), calls=%async_computation.2 | async-start | bytes 3145728 | tf_op jit(solution)/shard_map/all_gather | solution.py:85
  6.5 4.2 %copy-start.6 = (bf16[256,128]{1,0:T(8,128)(2,1)S(1)}, bf16[256,128]{1,0:T(8,128)(2,1)}, u32[]{:S(2)}) copy-start(bf16[256,128]{1,0:T(8,128)(2,1)} %param.25) | copy-start | bytes 196612
  8.1 8.7 %copy-start.12 = (bf16[16,128]{1,0:T(8,128)(2,1)S(1)}, bf16[16,128]{1,0:T(8,128)(2,1)}, u32[]{:S(2)}) copy-start(bf16[16,128]{1,0:T(8,128)(2,1)} %param.22) | copy-start | bytes 12292
  8.1 8.7 %copy-start.13 = (f32[128]{0:T(128)S(1)}, f32[128]{0:T(128)}, u32[]{:S(2)}) copy-start(f32[128]{0:T(128)} %param.23) | copy-start | bytes 1540
  10.7 132.1 %all-gather.9.cloned.1.call-start = ((), (), s32[]{:S(2)}) async-start(), calls=%async_computation.3 | async-start | bytes 1179648 | tf_op jit(solution)/shard_map/all_gather | solution.py:108
  13.0 4.6 %copy-start.8 = (bf16[128,128]{1,0:T(8,128)(2,1)S(1)}, bf16[128,128]{1,0:T(8,128)(2,1)}, u32[]{:S(2)}) copy-start(bf16[128,128]{1,0:T(8,128)(2,1)} %param.19) | copy-start | bytes 98308
  14.6 35.6 %copy-start.9 = (bf16[128,128]{1,0:T(8,128)(2,1)S(1)}, bf16[128,128]{1,0:T(8,128)(2,1)}, u32[]{:S(2)}) copy-start(bf16[128,128]{1,0:T(8,128)(2,1)} %param.18) | copy-start | bytes 98308
  14.6 66.6 %copy-start.7 = (bf16[128,256]{1,0:T(8,128)(2,1)S(1)}, bf16[128,256]{1,0:T(8,128)(2,1)}, u32[]{:S(2)}) copy-start(bf16[128,256]{1,0:T(8,128)(2,1)} %param.20) | copy-start | bytes 196612
  112.6 2.5 copy-start.2
  118.1 1.1 copy-start.4
  134.0 3.0 copy-start.5
  137.1 1.2 copy-start.11
  137.8 7.4 %copy-start.1 = (bf16[512,1024]{1,0:T(8,128)(2,1)S(1)}, bf16[512,1024]{1,0:T(8,128)(2,1)}, u32[]{:S(2)}) copy-start(bf16[512,1024]{1,0:T(8,128)(2,1)} %param.16) | copy-start | bytes 3145732
  139.2 5.2 %all-to-all-start = ((bf16[2,512,256]{1,2,0:T(8,128)(2,1)}), bf16[2,512,256]{1,2,0:T(8,128)(2,1)S(1)}, u32[]{:S(2)}, u32[]{:S(2)}) async-start(bf16[2,512,256]{1,2,0:T(8,128)(2,1)} %multiply_convert_fusion.2), calls=%async_computation | async-start | bytes 1048576 | tf_op jit(solution)/shard_map/all_to_all | solution.py:106
  142.7 18.0 %all-gather.11.cloned.1.call-start = ((), (), s32[]{:S(2)}) async-start(), calls=%async_computation.4 | async-start | bytes 3145728 | tf_op jit(solution)/shard_map/all_gather | solution.py:111
  144.4 0.8 copy-start.3
  145.2 2.2 copy-start.10
  148.7 72.5 %all-gather.13.cloned.1.call-start = ((), (), s32[]{:S(2)}) async-start(), calls=%async_computation.5 | async-start | bytes 3244032 | tf_op jit(solution)/shard_map/all_gather | solution.py:113
  149.3 129.9 %all-gather.15.cloned.1.call-start = ((), (), s32[]{:S(2)}) async-start(), calls=%async_computation.6 | async-start | bytes 3244032 | tf_op jit(solution)/shard_map/all_gather | solution.py:114
  149.9 189.5 %all-gather.17.cloned.1.call-start = ((), (), s32[]{:S(2)}) async-start(), calls=%async_computation.7 | async-start | bytes 3244032 | tf_op jit(solution)/shard_map/all_gather | solution.py:116
  150.4 210.1 %reduce-scatter.2.cloned.1.call-start = ((), (), s32[]{:S(2)}) async-start(), calls=%async_computation.8 | async-start | bytes 3145728 | tf_op jit(solution)/shard_map/reduce_scatter | solution.py:120
Sparse Core Ops, SparseCore 0:
  10.8 13.2 all-gather.6
  26.1 42.2 all-gather.8
  148.8 11.8 all-gather.10
  162.7 58.4 all-gather.12
  223.3 55.9 all-gather.14
  281.1 58.1 all-gather.16
  352.5 7.9 reduce-scatter.1
where the time goes:
time: 370 us
  waiting for transfers between devices  192 us (52%)
  blocking collectives  99.3 us (27%)
  matrix products  36.6 us (10%)
  other arithmetic  22.9 us (6%)
  between operations  13.8 us (4%)
  starting transfers between devices  3.91 us (1%)
    all_gather x1, waiting for transfers between devices, local(): lax.all_gather(gate_weight, 'fs', axis=0, tiled=True)  60.5 us
    all_gather x1, waiting for transfers between devices, local(): down_full = lax.all_gather(down_weight, 'fs', axis=1, tiled=True)  60.1 us
    all_gather x1, waiting for transfers between devices, local(): lax.all_gather(up_weight, 'fs', axis=0, tiled=True)  49.6 us
    all_gather x1, blocking collectives, local(): lax.all_gather(key_weight, 'fs', axis=0, tiled=True)  32.6 us
    all_gather x1, blocking collectives, local(): lax.all_gather(value_weight, 'fs', axis=0, tiled=True)  31.3 us
    all_gather x1, blocking collectives, local(): lax.all_gather(query_weight, 'fs', axis=0, tiled=True)  31.1 us
    dot_general x8, matrix products, project_inputs(): return jnp.dot(source, weight, preferred_element_type=jnp.float32)  29.6 us
    dynamic_update_slice x16, other arithmetic, linear_attention(): earlier = lax.scan(advance, initial, (lasting, update))[1]  10.6 us
  transfers between devices with their start and end apart: 8, of which 6 were waited for; matrix products, arithmetic and copies ran while one was open for 10% of the time, Pallas kernels for 0%

commit v1 on v0

--- a/solution.py
+++ b/solution.py
@@ -1,3 +1,4 @@
+import functools
 import jax
 import jax.numpy as jnp
 from jax import lax
@@ -9,6 +10,14 @@
 epsilon = 1e-06
 decay_softness = 16.0
 highest = lax.Precision.HIGHEST
+
+
+def time_quarters_up(panel, link_axis):
+    field_out = jax.lax.all_gather(panel, axis_name=link_axis)
+    return jnp.concatenate(field_out, axis=1)
+
+
+settle_slabs_on = functools.partial(time_quarters_up, link_axis="fs")
 
 
 def rms_scale(values, gains):
@@ -113,7 +122,7 @@
         lax.all_gather(gate_weight, "fs", axis=0, tiled=True),
         lax.all_gather(up_weight, "fs", axis=0, tiled=True),
     )
-    down_full = lax.all_gather(down_weight, "fs", axis=1, tiled=True)
+    down_full = settle_slabs_on(down_weight)
     hidden = (
         jax.nn.silu(project_inputs(ffn_sequence, gate_full)) * project_inputs(ffn_sequence, up_full)
     ).astype(jnp.bfloat16)

time: 370 us -> 313 us (0.85)
  waiting for transfers between devices: 192 us -> 129 us
  local copies, waits for them, and re-layouts: 1.33 us -> 5.89 us
    all_gather x1, waiting for transfers between devices: 60.1 us -> 0.02 us  [time_quarters_up(): field_out = jax.lax.all_gather(panel, axis_name=link_axis)]
    reshape x0 -> x1, local copies, waits for them, and re-layouts: none -> 4.56 us  [time_quarters_up(): return jnp.concatenate(field_out, axis=1)]
  transfers between devices with their start and end apart: 8 -> 8, of which waited for: 6 -> 5; matrix products, arithmetic and copies ran while one was open for 10% -> 14% of each run, Pallas kernels for 0% -> 0%
where the time goes in v1:
time: 313 us
  waiting for transfers between devices  129 us (41%)
  blocking collectives  101 us (32%)
  matrix products  36.7 us (12%)
  other arithmetic  22.9 us (7%)
  between operations  13.8 us (4%)
  local copies, waits for them, and re-layouts  5.89 us (2%)
  starting transfers between devices  3.92 us (1%)
    all_gather x1, waiting for transfers between devices, local(): lax.all_gather(gate_weight, 'fs', axis=0, tiled=True)  60.5 us
    all_gather x1, waiting for transfers between devices, local(): lax.all_gather(up_weight, 'fs', axis=0, tiled=True)  49.7 us
    all_gather x1, blocking collectives, local(): lax.all_gather(value_weight, 'fs', axis=0, tiled=True)  32.9 us
    all_gather x1, blocking collectives, local(): lax.all_gather(key_weight, 'fs', axis=0, tiled=True)  32.5 us
    all_gather x1, blocking collectives, local(): lax.all_gather(query_weight, 'fs', axis=0, tiled=True)  31.3 us
    dot_general x8, matrix products, project_inputs(): return jnp.dot(source, weight, preferred_element_type=jnp.float32)  29.6 us
    dynamic_update_slice x16, other arithmetic, linear_attention(): earlier = lax.scan(advance, initial, (lasting, update))[1]  10.6 us
    reduce_scatter x1, waiting for transfers between devices, local(): lax.psum_scatter(project_inputs(hidden, down_full).astype(jnp.bfloat16),...  8.51 us
  transfers between devices with their start and end apart: 8, of which 5 were waited for; matrix products, arithmetic and copies ran while one was open for 14% of the time, Pallas kernels for 0%

profile of v1, /device:TPU:0, one launch (start us, length us, event | category | flops | bytes accessed | tf_op | source)
XLA Modules:
  0.0 312.8 jit_solution(3237864823844066380)
XLA Ops:
  6.5 1.5 fusion.2
  8.1 2.5 fusion.4
  10.7 2.2 all_gather.41
  13.0 0.7 all-gather.18.cloned.1.call-update
  13.7 1.6 convolution_convert_fusion.3
  15.4 1.8 all_gather.39
  17.2 0.5 fusion.12
  17.7 0.3 fusion.24
  18.1 32.5 %all_gather.40 = bf16[1024,128]{1,0:T(8,128)(2,1)S(1)} all-gather(bf16[128,128]{1,0:T(8,128)(2,1)S(1)} %copy-done.8), channel_id=1, replica_groups=mesh['rep'=2,'fs'=8,'tp'=2] {'fs'}, dimensions={0}, use_global_device_ids=true | all-gather | bytes 294912 | tf_op jit(solution)/shard_map/all_gather | solution.py:100
  50.5 31.3 %all_gather.38 = bf16[1024,128]{1,0:T(8,128)(2,1)S(1)} all-gather(bf16[128,128]{1,0:T(8,128)(2,1)S(1)} %copy-done.9), channel_id=1, replica_groups=mesh['rep'=2,'fs'=8,'tp'=2] {'fs'}, dimensions={0}, use_global_device_ids=true | all-gather | bytes 294912 | tf_op jit(solution)/shard_map/all_gather | solution.py:99
  81.8 32.9 %all_gather.37 = bf16[1024,256]{1,0:T(8,128)(2,1)S(1)} all-gather(bf16[128,256]{1,0:T(8,128)(2,1)S(1)} %copy-done.7), channel_id=1, replica_groups=mesh['rep'=2,'fs'=8,'tp'=2] {'fs'}, dimensions={0}, use_global_device_ids=true | all-gather | bytes 589824 | tf_op jit(solution)/shard_map/all_gather | solution.py:101
  114.7 2.4 convolution_convert_fusion.1
  117.2 0.7 convolution_convert_fusion.2
  118.0 1.6 fusion.14
  119.5 0.7 convolution_convert_fusion
  120.3 1.1 convolution_bitcast_fusion
  121.4 12.6 %while.13 = (s32[]{:T(128)}, f32[1,128,256]{2,1,0:T(8,128)S(1)}, f32[16,1,128,256]{3,2,1,0:T(8,128)}, f32[16,1,128]{2,1,0:T(1,128)S(1)}, f32[16,1,128,256]{3,2,1,0:T(8,128)S(1)}, /*index=5*/s32[]{:T(128)}, s32[]{:T(128)}) while((s32[]{:T(128)}, f32[1,128,256]{2,1,0:T(8,128)S(1)}, f32[16,1,128,256]{3,2,1,0:T(8,128)}, ...), condition=%wide.region_3.4_spmd.clone, body=%wide.region_2.3_spmd.clone.sunk | while | flops 131075 | bytes 657504 | solution.py:63
  121.4 0.7 bitcast_dynamic-update-slice_fusion.2
  122.0 0.1 bitcast_add_fusion.2
  122.2 0.7 bitcast_dynamic-update-slice_fusion.2
  122.8 0.1 bitcast_add_fusion.2
  123.0 0.7 bitcast_dynamic-update-slice_fusion.2
  123.6 0.1 bitcast_add_fusion.2
  123.7 0.7 bitcast_dynamic-update-slice_fusion.2
  124.5 0.7 bitcast_dynamic-update-slice_fusion.2
  125.2 0.1 bitcast_add_fusion.2
  125.3 0.7 bitcast_dynamic-update-slice_fusion.2
  126.0 0.1 bitcast_add_fusion.2
  126.1 0.7 bitcast_dynamic-update-slice_fusion.2
  126.8 0.1 bitcast_add_fusion.2
  126.9 0.7 bitcast_dynamic-update-slice_fusion.2
  127.6 0.1 bitcast_add_fusion.2
  127.7 0.7 bitcast_dynamic-update-slice_fusion.2
  128.5 0.7 bitcast_dynamic-update-slice_fusion.2
  129.2 0.1 bitcast_add_fusion.2
  129.3 0.7 bitcast_dynamic-update-slice_fusion.2
  129.9 0.1 bitcast_add_fusion.2
  130.1 0.7 bitcast_dynamic-update-slice_fusion.2
  130.9 0.6 bitcast_dynamic-update-slice_fusion.2
  131.5 0.1 bitcast_add_fusion.2
  131.6 0.7 bitcast_dynamic-update-slice_fusion.2
  132.4 0.7 bitcast_dynamic-update-slice_fusion.2
  133.2 0.7 bitcast_dynamic-update-slice_fusion.2
  134.0 2.2 convolution_select_fusion
  136.3 3.0 fusion.5
  139.3 0.7 fusion.10
  140.0 0.3 copy.45
  140.5 0.9 multiply_convert_fusion.2
  141.4 3.5 %all-to-all-start = ((bf16[2,512,256]{1,2,0:T(8,128)(2,1)}), bf16[2,512,256]{1,2,0:T(8,128)(2,1)S(1)}, u32[]{:S(2)}, u32[]{:S(2)}) async-start(bf16[2,512,256]{1,2,0:T(8,128)(2,1)} %multiply_convert_fusion.2), calls=%async_computation | async-start | bytes 1048576 | tf_op jit(solution)/shard_map/all_to_all | solution.py:115
  145.0 1.7 all-to-all-done
  146.6 0.8 copy-done.3
  147.4 2.2 multiply_reduce_fusion
  149.7 1.2 multiply_convert_fusion.1
  151.0 0.5 all-gather.14.cloned.1.call-update
  151.5 0.5 all-gather.16.cloned.1.call-update
  152.1 0.2 reduce-scatter.2.cloned.1.call-start
  152.3 4.6 %copy.46 = bf16[1408,8,128]{0,2,1:T(8,128)(2,1)} copy(bf16[1408,8,128]{2,0,1:T(8,128)(2,1)} %bitcast.87) | data formatting | bytes 5767168 | tf_op jit(solution)/shard_map/reshape | solution.py:17
  156.9 6.4 %all-gather.12.cloned.1.call-done = bf16[1024,1024]{1,0:T(8,128)(2,1)} async-done(((bf16[512,1024]{1,0:T(8,128)(2,1)}), bf16[1024,1024]{1,0:T(8,128)(2,1)}) %all-gather.12.cloned.1.call-update) | async-done | bytes 2097168 | tf_op jit(solution)/shard_map/all_gather | solution.py:120
  163.3 60.5 %all-gather.14.cloned.1.call-done = bf16[1024,1408]{1,0:T(8,128)(2,1)} async-done(((bf16[128,1408]{1,0:T(8,128)(2,1)}), bf16[1024,1408]{1,0:T(8,128)(2,1)}) %all-gather.14.cloned.1.call-update) | async-done | bytes 2883600 | tf_op jit(solution)/shard_map/all_gather | solution.py:122
  223.8 8.3 %fusion.27 = f32[1024,1408]{1,0:T(8,128)} fusion(bf16[1024,1024]{1,0:T(8,128)(2,1)} %all-gather.12.cloned.1.call-done, bf16[1024,1408]{1,0:T(8,128)(2,1)} %all-gather.14.cloned.1.call-done), kind=kOutput, calls=%fused_computation.58 | convolution fusion | flops 2952790016 | bytes 10747904 | tf_op jit(solution)/shard_map/dot_general | solution.py:71
  232.2 49.7 %all-gather.16.cloned.1.call-done = bf16[1024,1408]{1,0:T(8,128)(2,1)} async-done(((bf16[128,1408]{1,0:T(8,128)(2,1)}), bf16[1024,1408]{1,0:T(8,128)(2,1)}) %all-gather.16.cloned.1.call-update) | async-done | bytes 2883600 | tf_op jit(solution)/shard_map/all_gather | solution.py:123
  281.8 13.1 %fusion.8 = bf16[1024,1024]{1,0:T(8,128)(2,1)} fusion(bf16[1408,1024]{0,1:T(8,128)(2,1)} %bitcast.88, f32[1024,1408]{1,0:T(8,128)} %fusion.27, bf16[1024,1024]{1,0:T(8,128)(2,1)} %all-gather.12.cloned.1.call-done, bf16[1024,1408]{1,0:T(8,128)(2,1)} %all-gather.16.cloned.1.call-done), kind=kOutput, calls=%fused_computation.18 | convolution fusion | flops 5915279360 | bytes 15728640 | tf_op jit(solution)/shard_map/dot_general | solution.py:71
  294.9 8.5 %reduce-scatter.2.cloned.1.call-done = bf16[512,1024]{1,0:T(8,128)(2,1)} async-done(((bf16[1024,1024]{1,0:T(8,128)(2,1)}), bf16[512,1024]{1,0:T(8,128)(2,1)}) %reduce-scatter.2.cloned.1.call-update) | async-done | bytes 1048592 | tf_op jit(solution)/shard_map/reduce_scatter | solution.py:129
  303.4 2.5 add_convert_fusion
  (72 shorter events, 1.2 us)
Async XLA Ops:
  6.5 7.2 %copy-start = (bf16[1024,16]{0,1:T(8,128)(2,1)S(1)}, bf16[1024,16]{0,1:T(8,128)(2,1)}, u32[]{:S(2)}) copy-start(bf16[1024,16]{0,1:T(8,128)(2,1)} %param.21) | copy-start | bytes 98308
  6.5 108.2 %all-gather.8.cloned.1.call-start = ((), (), s32[]{:S(2)}) async-start(), calls=%async_computation.2 | async-start | bytes 3145728 | tf_op jit(solution)/shard_map/all_gather | solution.py:94
  6.5 4.2 %copy-start.6 = (bf16[256,128]{1,0:T(8,128)(2,1)S(1)}, bf16[256,128]{1,0:T(8,128)(2,1)}, u32[]{:S(2)}) copy-start(bf16[256,128]{1,0:T(8,128)(2,1)} %param.25) | copy-start | bytes 196612
  8.1 9.1 %copy-start.12 = (bf16[16,128]{1,0:T(8,128)(2,1)S(1)}, bf16[16,128]{1,0:T(8,128)(2,1)}, u32[]{:S(2)}) copy-start(bf16[16,128]{1,0:T(8,128)(2,1)} %param.22) | copy-start | bytes 12292
  8.1 9.1 %copy-start.13 = (f32[128]{0:T(128)S(1)}, f32[128]{0:T(128)}, u32[]{:S(2)}) copy-start(f32[128]{0:T(128)} %param.23) | copy-start | bytes 1540
  10.7 134.3 %all-gather.10.cloned.1.call-start = ((), (), s32[]{:S(2)}) async-start(), calls=%async_computation.3 | async-start | bytes 1179648 | tf_op jit(solution)/shard_map/all_gather | solution.py:117
  12.9 5.1 %copy-start.8 = (bf16[128,128]{1,0:T(8,128)(2,1)S(1)}, bf16[128,128]{1,0:T(8,128)(2,1)}, u32[]{:S(2)}) copy-start(bf16[128,128]{1,0:T(8,128)(2,1)} %param.19) | copy-start | bytes 98308
  12.9 139.4 %all-gather.18.cloned.1.call-start = ((), (), s32[]{:S(2)}) async-start(), calls=%async_computation.8 | async-start | bytes 3244032 | tf_op jit(solution)/shard_map/all_gather | solution.py:16
  13.7 36.9 %copy-start.9 = (bf16[128,128]{1,0:T(8,128)(2,1)S(1)}, bf16[128,128]{1,0:T(8,128)(2,1)}, u32[]{:S(2)}) copy-start(bf16[128,128]{1,0:T(8,128)(2,1)} %param.18) | copy-start | bytes 98308
  13.7 68.1 %copy-start.7 = (bf16[128,256]{1,0:T(8,128)(2,1)S(1)}, bf16[128,256]{1,0:T(8,128)(2,1)}, u32[]{:S(2)}) copy-start(bf16[128,256]{1,0:T(8,128)(2,1)} %param.20) | copy-start | bytes 196612
  114.7 2.5 copy-start.2
  120.3 1.1 copy-start.4
  136.3 3.0 copy-start.5
  139.3 1.2 copy-start.11
  140.0 7.4 %copy-start.1 = (bf16[512,1024]{1,0:T(8,128)(2,1)S(1)}, bf16[512,1024]{1,0:T(8,128)(2,1)}, u32[]{:S(2)}) copy-start(bf16[512,1024]{1,0:T(8,128)(2,1)} %param.16) | copy-start | bytes 3145732
  141.4 5.2 %all-to-all-start = ((bf16[2,512,256]{1,2,0:T(8,128)(2,1)}), bf16[2,512,256]{1,2,0:T(8,128)(2,1)S(1)}, u32[]{:S(2)}, u32[]{:S(2)}) async-start(bf16[2,512,256]{1,2,0:T(8,128)(2,1)} %multiply_convert_fusion.2), calls=%async_computation | async-start | bytes 1048576 | tf_op jit(solution)/shard_map/all_to_all | solution.py:115
  144.9 18.4 %all-gather.12.cloned.1.call-start = ((), (), s32[]{:S(2)}) async-start(), calls=%async_computation.4 | async-start | bytes 3145728 | tf_op jit(solution)/shard_map/all_gather | solution.py:120
  146.6 0.8 copy-start.3
  147.4 2.2 copy-start.10
  150.9 72.9 %all-gather.14.cloned.1.call-start = ((), (), s32[]{:S(2)}) async-start(), calls=%async_computation.5 | async-start | bytes 3244032 | tf_op jit(solution)/shard_map/all_gather | solution.py:122
  151.5 130.3 %all-gather.16.cloned.1.call-start = ((), (), s32[]{:S(2)}) async-start(), calls=%async_computation.6 | async-start | bytes 3244032 | tf_op jit(solution)/shard_map/all_gather | solution.py:123
  152.1 151.3 %reduce-scatter.2.cloned.1.call-start = ((), (), s32[]{:S(2)}) async-start(), calls=%async_computation.7 | async-start | bytes 3145728 | tf_op jit(solution)/shard_map/reduce_scatter | solution.py:129
Sparse Core Ops, SparseCore 0:
  10.8 13.2 all-gather.7
  26.1 42.5 all-gather.9
  70.9 59.4 all-gather.17
  151.0 12.2 all-gather.11
  165.3 58.4 all-gather.13
  225.9 55.9 all-gather.15
  295.0 8.3 reduce-scatter.1
